TPU v7x, 32 devices: a whole 2x2x4 slice. The times are simulated.
32 devices in a mesh: dp: 4 (over y, x), kv: 4 (over z), tp: 2 (over core).
Axes of the slice: x: 2, y: 2, z: 4, core: 2. Of those that a mesh axis runs over, the one named last changes fastest.
Arguments:
- tokens: bfloat16 [4, 1024, 1024], P('dp', 'kv', 'tp'), may hold values from -6 to 6
- norm_gain: float32 [1024], replicated, may hold values from 0.1 to 1.9
- w_query: bfloat16 [1024, 1024], P(None, 'tp'), may hold values from -0.1875 to 0.1875
- w_key: bfloat16 [1024, 256], P(None, 'tp'), may hold values from -0.1875 to 0.1875
- w_value: bfloat16 [1024, 256], P(None, 'tp'), may hold values from -0.1875 to 0.1875
- q_gain: float32 [64], replicated, may hold values from 0.1 to 1.9
- k_gain: float32 [64], replicated, may hold values from 0.1 to 1.9
- w_out: bfloat16 [1024, 1024], P('tp'), may hold values from -4 to 4
- chosen: int32 [4, 32, 16], P('dp', 'kv'), may hold values from -1 to 31, as said below
Outputs:
- mixed: bfloat16 [4, 1024, 1024], P('dp', 'kv', 'tp')
- log_total: float32 [4, 16, 1024], P('dp', 'tp', 'kv')
Inputs may be any that keep to these rules, and one draw needn't show every extreme that they name: Each row of chosen (one query block b) holds distinct key block numbers, all at most b, and -1 for empty entries; b itself is always present; a row is full (16 blocks) whenever at least 16 blocks may be chosen by it. Over the 8 rows of one index of kv, the chosen blocks that lie on any one other index of kv are at most 4 distinct ones, and exactly 4 of those on the index just before, for every index but the first. Some blocks are chosen far more often than others.
All inputs are finite; a program needn't handle non-finite values.
Results may differ from a plain program's by a relative error of at most 0.015.
Values may be sent and summed in bfloat16 or wider, within the bound.
A program may use at most 64 MiB of HBM per device.

v0:
```python
import math
import jax
import jax.numpy as jnp
from jax import lax
from jax.sharding import PartitionSpec as P

H = 16
HD = 64
BLK = 32
epsilon = 1e-06
alibi_reach = 4.0
masked = -1e30


def rms_norm(values, gain):
    return (
        values
        * lax.rsqrt(jnp.mean(values * values, axis=-1, keepdims=True) + epsilon)
        * gain.astype(jnp.float32)
    )


def shards(tokens, norm_gain, w_query, w_key, w_value, q_gain, k_gain, w_out, chosen):
    gathered = lax.all_gather(tokens, "tp", axis=2, tiled=True)
    seq_dev, tok_dev, model_width = gathered.shape
    n_kv = lax.axis_size("kv")
    n_tp = lax.axis_size("tp")
    kv_index = lax.axis_index("kv")
    tp_index = lax.axis_index("tp")
    heads_here = w_query.shape[1] // HD
    kv_here = w_key.shape[1] // HD
    group_size = heads_here // kv_here
    blocks_here = tok_dev // BLK
    seq_len = tok_dev * n_kv
    hidden = (
        rms_norm(gathered.astype(jnp.float32), norm_gain)
        .astype(jnp.bfloat16)
        .reshape(seq_dev * tok_dev, model_width)
    )
    queries = rms_norm(
        jnp.dot(hidden, w_query, preferred_element_type=jnp.float32).reshape(
            seq_dev, tok_dev, heads_here, HD
        ),
        q_gain,
    ).astype(jnp.bfloat16)
    key_rows = rms_norm(
        jnp.dot(hidden, w_key, preferred_element_type=jnp.float32).reshape(
            seq_dev, tok_dev, kv_here, HD
        ),
        k_gain,
    ).astype(jnp.bfloat16)
    value_rows = (
        jnp.dot(hidden, w_value, preferred_element_type=jnp.float32)
        .astype(jnp.bfloat16)
        .reshape(seq_dev, tok_dev, kv_here, HD)
    )
    queries = queries.reshape(seq_dev, blocks_here, BLK, kv_here, group_size, HD)
    head_ids = tp_index * heads_here + jnp.arange(heads_here, dtype=jnp.int32)
    slopes = jnp.exp2(-8.0 * (head_ids + 1).astype(jnp.float32) / H).reshape(kv_here, group_size)
    query_pos = (kv_index * tok_dev + jnp.arange(tok_dev, dtype=jnp.int32)).reshape(
        blocks_here, BLK
    )
    score_scale = HD ** (-0.5)

    def absorb(state_now, span_keys, span_values, key_pos, usable):
        row_max, row_sum, weighted = state_now
        key_block = key_pos // BLK
        member = jnp.any(chosen[:, :, :, None] == key_block[:, None, None, :], axis=2)
        offset = query_pos[None, :, :, None] - key_pos[:, None, None, :]
        allowed = member[:, :, None, :] & usable[:, None, None, :] & (offset >= 0)
        scores = (
            jnp.einsum(
                "sbqkgd,snkd->skgbqn", queries, span_keys, preferred_element_type=jnp.float32
            )
            * score_scale
        )
        penalty = (
            slopes[None, :, :, None, None, None]
            * offset.astype(jnp.float32)[:, None, None]
            * alibi_reach
            / seq_len
        )
        scores = jnp.where(allowed[:, None, None], scores - penalty, masked)
        new_max = jnp.maximum(row_max, jnp.max(scores, axis=-1))
        weights = jnp.where(allowed[:, None, None], jnp.exp(scores - new_max[..., None]), 0.0)
        shrink = jnp.exp(row_max - new_max)
        row_sum = row_sum * shrink + jnp.sum(weights, axis=-1)
        weighted = weighted * shrink[..., None] + jnp.einsum(
            "skgbqn,snkd->skgbqd",
            weights.astype(jnp.bfloat16),
            span_values,
            preferred_element_type=jnp.float32,
        )
        return (new_max, row_sum, weighted)

    stat_shape = (seq_dev, kv_here, group_size, blocks_here, BLK)
    initial = (
        jnp.full(stat_shape, masked, jnp.float32),
        jnp.zeros(stat_shape, jnp.float32),
        jnp.zeros(stat_shape + (HD,), jnp.float32),
    )

    def fold_piece(state_now, shard_piece, first_row):
        piece_keys, piece_values = shard_piece
        row_count = piece_keys.shape[1]
        span_len = math.gcd(row_count, tok_dev)

        def one_span(step_index, running):
            first_key = step_index * span_len
            span_keys = lax.dynamic_slice_in_dim(piece_keys, first_key, span_len, 1)
            span_values = lax.dynamic_slice_in_dim(piece_values, first_key, span_len, 1)
            key_pos = jnp.broadcast_to(
                first_row.astype(jnp.int32) + first_key + jnp.arange(span_len, dtype=jnp.int32),
                (seq_dev, span_len),
            )
            return absorb(
                running, span_keys, span_values, key_pos, jnp.ones((seq_dev, span_len), bool)
            )

        return lax.fori_loop(0, row_count // span_len, one_span, state_now)

    row_max, row_sum, weighted = fold_piece(
        initial,
        (
            lax.all_gather(key_rows, "kv", axis=1, tiled=True),
            lax.all_gather(value_rows, "kv", axis=1, tiled=True),
        ),
        jnp.int32(0),
    )
    attended = (weighted / row_sum[..., None]).transpose(0, 3, 4, 1, 2, 5)
    attended = attended.reshape(seq_dev * tok_dev, heads_here * HD).astype(jnp.bfloat16)
    log_total = (row_max + jnp.log(row_sum)).reshape(seq_dev, heads_here, tok_dev)
    own_rows = model_width // n_tp

    def project():
        out_cols = lax.slice_in_dim(w_out, 0, own_rows * lax.axis_size("tp"), axis=1)
        return jnp.dot(attended, out_cols, preferred_element_type=jnp.float32).T

    scattered = lax.psum_scatter(
        project().astype(jnp.bfloat16), "tp", scatter_dimension=0, tiled=True
    ).astype(jnp.float32)
    mixed = scattered.T.reshape(seq_dev, tok_dev, own_rows).astype(jnp.bfloat16)
    return (mixed, log_total)


def solution(mesh):
    in_specs = (
        P("dp", "kv", "tp"),
        P(),
        P(None, "tp"),
        P(None, "tp"),
        P(None, "tp"),
        P(),
        P(),
        P("tp", None),
        P("dp", "kv", None),
    )
    out_specs = (P("dp", "kv", "tp"), P("dp", "tp", "kv"))
    return jax.shard_map(shards, mesh=mesh, in_specs=in_specs, out_specs=out_specs, check_vma=False)
```

profile of v0, /device:TPU:0, one launch (start us, length us, event | category | flops | bytes accessed | tf_op | source)
XLA Modules:
  0.0 81.3 jit_solution(10249953948225324526)
XLA Ops:
  7.3 2.6 %all_gather.9 = bf16[1,256,1024]{2,1,0:T(8,128)(2,1)S(1)} all-gather(bf16[1,256,512]{2,1,0:T(8,128)(2,1)} %param.11), channel_id=1, replica_groups=mesh['dp'=4,'kv'=4,'tp'=2] {'tp'}, dimensions={2}, use_global_device_ids=true | all-gather | bytes 786432 | tf_op jit(solution)/shard_map/all_gather | solution.py:24
  9.9 0.2 fusion.20
  10.1 1.4 %convolution_convert_fusion.1 = bf16[256,128]{0,1:T(8,128)(2,1)S(1)} fusion(bf16[1024,128]{1,0:T(8,128)(2,1)} %param.15, bf16[1,256,1024]{2,1,0:T(8,128)(2,1)S(1)} %all_gather.9, f32[1024]{0:T(1024)} %param.12, f32[256]{0:T(256)S(1)} %add_rsqrt_fusion.2), kind=kOutput, calls=%fused_computation.39 | convolution fusion | flops 68190208 | bytes 857088 | tf_op jit(solution)/shard_map/dot_general | solution.py:53
  11.5 0.4 fusion.30
  12.0 0.1 multiply_convert_fusion
  12.0 16.2 %all_gather.10 = bf16[1,1024,2,64]{1,3,2,0:T(8,128)(2,1)} all-gather(bf16[1,256,2,64]{1,3,2,0:T(8,128)(2,1)S(1)} %multiply_convert_fusion), channel_id=1, replica_groups=mesh['dp'=4,'kv'=4,'tp'=2] {'kv'}, dimensions={1}, use_global_device_ids=true | all-gather | bytes 327680 | tf_op jit(solution)/shard_map/all_gather | solution.py:125
  28.2 14.6 %all_gather.11 = bf16[1,1024,2,64]{1,3,2,0:T(8,128)(2,1)S(1)} all-gather(bf16[1,256,2,64]{1,3,2,0:T(8,128)(2,1)S(1)} %bitcast.99), channel_id=1, replica_groups=mesh['dp'=4,'kv'=4,'tp'=2] {'kv'}, dimensions={1}, use_global_device_ids=true | all-gather | bytes 327680 | tf_op jit(solution)/shard_map/all_gather | solution.py:126
  42.8 1.3 %fusion.33 = (f32[256,512]{1,0:T(8,128)S(1)}, f32[256,512]{1,0:T(8,128)}) fusion(bf16[1024,512]{1,0:T(8,128)(2,1)S(1)} %copy-done, bf16[1,256,1024]{2,1,0:T(8,128)(2,1)S(1)} %all_gather.9, f32[1024]{0:T(1024)S(1)} %copy-done.3, f32[256]{0:T(256)S(1)} %add_rsqrt_fusion.2), kind=kOutput, calls=%fused_computation.59 | convolution fusion | flops 269615104 | bytes 2626560 | tf_op jit(solution)/shard_map/dot_general | solution.py:41
  44.1 0.2 copy.26
  44.5 1.6 %reshape.336 = f32[1,8,32,2,4,64]{5,4,3,2,1,0:T(4,128)S(1)} reshape(f32[256,512]{1,0:T(8,128)} %get-tuple-element.319) | data formatting | bytes 1048576 | tf_op jit(solution)/shard_map/reshape | solution.py:41
  46.1 1.1 %fusion.24 = bf16[1,8,32,2,4,64]{5,2,4,1,3,0:T(8,128)(2,1)} fusion(f32[1,8,32,2,4,64]{5,4,3,2,1,0:T(4,128)S(1)} %reshape.336, f32[64]{0:T(128)S(1)} %copy-done.5, f32[8,32,2,4]{1,3,0,2:T(4,128)S(1)} %copy.27), kind=kLoop, calls=%fused_computation.45 | loop fusion | flops 393216 | bytes 794880 | tf_op jit(solution)/shard_map/convert_element_type | solution.py:45
  47.2 15.7 %while.20 = (s32[]{:T(128)}, f32[1,2,4,8,32]{4,2,3,1,0:T(4,128)S(1)}, f32[1,2,4,8,32]{4,2,3,1,0:T(4,128)S(1)}, f32[1,2,4,8,32,64]{5,4,3,2,1,0:T(8,128)S(1)}, s32...) while((s32[]{:T(128)}, ...), condition=%wide.region_7.8_spmd.clone, body=%wide.region_3.7_spmd.clone.sunk | while | flops 140261664 | bytes 9419611 | solution.py:120
  47.2 0.1 mul.331
  47.3 0.1 compare_reduce_fusion.2
  47.5 0.1 fusion.48
  47.7 0.1 subtract_convert_fusion.2
  47.8 1.7 %fusion.49 = (f32[2,4,8,32]{3,1,2,0:T(4,128)S(1)}, f32[1,2,4,8,32,256]{5,4,2,3,1,0:T(8,128)S(1)}) fusion(f32[8,32,256]{2,1,0:T(8,128)S(1)} %subtract_convert_fusion.2, f32[2,4]{1,0:T(2,128)S(1)} %mul.331, bf16[1,8,32,2,4,64]{5,2,4,1,3,0:T(8,128)(2,1)} %get-tuple-element.431, bf16[1,1024,2,64]{1,3,2,0:T(8,128)(2,1)} %get-tuple-element.430, ...), kind=kOutput, calls=%fused_computation.58.clone.1 | convolution fusion | flops 70252544 | bytes 3022884 | tf_op jit(solution)/shard_map/while/body/eval_jaxpr/sbqkgd,snkd->skgbqn/dot_general | solution.py:72
  49.6 0.8 %fusion.51 = (bf16[2,4,8,32,256]{4,3,1,2,0:T(8,128)(2,1)S(1)}, f32[2,4,8,32]{3,1,2,0:T(4,128)S(1)}) fusion(f32[1,2,4,8,32,256]{5,4,2,3,1,0:T(8,128)S(1)} %get-tuple-element.393, f32[2,4,8,32]{3,1,2,0:T(4,128)S(1)} %bitcast.92, pred[8,32,256]{2,1,0:T(8,128)(4,1)S(1)} %fusion.48), kind=kLoop, calls=%fused_computation.9.clone.1 | loop fusion | flops 2095104 | bytes 3227648 | tf_op jit(solution)/shard_map/reshape.263
  50.4 0.7 fusion.52
  51.2 0.1 mul.331
  51.3 0.1 compare_reduce_fusion.2
  51.4 0.1 sub.166
  51.5 0.1 fusion.48
  51.6 0.1 subtract_convert_fusion.2
  51.7 1.7 %fusion.49 = (f32[2,4,8,32]{3,1,2,0:T(4,128)S(1)}, f32[1,2,4,8,32,256]{5,4,2,3,1,0:T(8,128)S(1)}) fusion(f32[8,32,256]{2,1,0:T(8,128)S(1)} %subtract_convert_fusion.2, f32[2,4]{1,0:T(2,128)S(1)} %mul.331, bf16[1,8,32,2,4,64]{5,2,4,1,3,0:T(8,128)(2,1)} %get-tuple-element.431, bf16[1,1024,2,64]{1,3,2,0:T(8,128)(2,1)} %get-tuple-element.430, ...), kind=kOutput, calls=%fused_computation.58.clone.1 | convolution fusion | flops 70252544 | bytes 3022884 | tf_op jit(solution)/shard_map/while/body/eval_jaxpr/sbqkgd,snkd->skgbqn/dot_general | solution.py:72
  53.5 0.8 %fusion.51 = (bf16[2,4,8,32,256]{4,3,1,2,0:T(8,128)(2,1)S(1)}, f32[2,4,8,32]{3,1,2,0:T(4,128)S(1)}) fusion(f32[1,2,4,8,32,256]{5,4,2,3,1,0:T(8,128)S(1)} %get-tuple-element.393, f32[2,4,8,32]{3,1,2,0:T(4,128)S(1)} %bitcast.92, pred[8,32,256]{2,1,0:T(8,128)(4,1)S(1)} %fusion.48), kind=kLoop, calls=%fused_computation.9.clone.1 | loop fusion | flops 2095104 | bytes 3227648 | tf_op jit(solution)/shard_map/reshape.263
  54.4 0.6 fusion.52
  55.1 0.1 mul.331
  55.2 0.1 compare_reduce_fusion.2
  55.4 0.1 fusion.48
  55.5 0.1 subtract_convert_fusion.2
  55.6 1.7 %fusion.49 = (f32[2,4,8,32]{3,1,2,0:T(4,128)S(1)}, f32[1,2,4,8,32,256]{5,4,2,3,1,0:T(8,128)S(1)}) fusion(f32[8,32,256]{2,1,0:T(8,128)S(1)} %subtract_convert_fusion.2, f32[2,4]{1,0:T(2,128)S(1)} %mul.331, bf16[1,8,32,2,4,64]{5,2,4,1,3,0:T(8,128)(2,1)} %get-tuple-element.431, bf16[1,1024,2,64]{1,3,2,0:T(8,128)(2,1)} %get-tuple-element.430, ...), kind=kOutput, calls=%fused_computation.58.clone.1 | convolution fusion | flops 70252544 | bytes 3022884 | tf_op jit(solution)/shard_map/while/body/eval_jaxpr/sbqkgd,snkd->skgbqn/dot_general | solution.py:72
  57.4 0.8 %fusion.51 = (bf16[2,4,8,32,256]{4,3,1,2,0:T(8,128)(2,1)S(1)}, f32[2,4,8,32]{3,1,2,0:T(4,128)S(1)}) fusion(f32[1,2,4,8,32,256]{5,4,2,3,1,0:T(8,128)S(1)} %get-tuple-element.393, f32[2,4,8,32]{3,1,2,0:T(4,128)S(1)} %bitcast.92, pred[8,32,256]{2,1,0:T(8,128)(4,1)S(1)} %fusion.48), kind=kLoop, calls=%fused_computation.9.clone.1 | loop fusion | flops 2095104 | bytes 3227648 | tf_op jit(solution)/shard_map/reshape.263
  58.3 0.6 fusion.52
  59.0 0.1 mul.331
  59.1 0.1 compare_reduce_fusion.2
  59.3 0.1 fusion.48
  59.4 0.1 subtract_convert_fusion.2
  59.5 1.7 %fusion.49 = (f32[2,4,8,32]{3,1,2,0:T(4,128)S(1)}, f32[1,2,4,8,32,256]{5,4,2,3,1,0:T(8,128)S(1)}) fusion(f32[8,32,256]{2,1,0:T(8,128)S(1)} %subtract_convert_fusion.2, f32[2,4]{1,0:T(2,128)S(1)} %mul.331, bf16[1,8,32,2,4,64]{5,2,4,1,3,0:T(8,128)(2,1)} %get-tuple-element.431, bf16[1,1024,2,64]{1,3,2,0:T(8,128)(2,1)} %get-tuple-element.430, ...), kind=kOutput, calls=%fused_computation.58.clone.1 | convolution fusion | flops 70252544 | bytes 3022884 | tf_op jit(solution)/shard_map/while/body/eval_jaxpr/sbqkgd,snkd->skgbqn/dot_general | solution.py:72
  61.3 0.8 %fusion.51 = (bf16[2,4,8,32,256]{4,3,1,2,0:T(8,128)(2,1)S(1)}, f32[2,4,8,32]{3,1,2,0:T(4,128)S(1)}) fusion(f32[1,2,4,8,32,256]{5,4,2,3,1,0:T(8,128)S(1)} %get-tuple-element.393, f32[2,4,8,32]{3,1,2,0:T(4,128)S(1)} %bitcast.92, pred[8,32,256]{2,1,0:T(8,128)(4,1)S(1)} %fusion.48), kind=kLoop, calls=%fused_computation.9.clone.1 | loop fusion | flops 2095104 | bytes 3227648 | tf_op jit(solution)/shard_map/reshape.263
  62.2 0.7 fusion.52
  62.9 0.3 fusion.26
  63.3 0.4 copy.30
  63.7 0.3 convert_element_type.92
  64.0 0.1 copy-done.1
  64.1 1.2 %fusion.19 = bf16[1024,256]{0,1:T(8,128)(2,1)} fusion(bf16[256,512]{1,0:T(8,128)(2,1)S(1)} %convert_element_type.92, bf16[512,1024]{1,0:T(8,128)(2,1)S(1)} %copy-done.1), kind=kOutput, calls=%fused_computation.38 | convolution fusion | flops 268697600 | bytes 1835008 | tf_op jit(solution)/shard_map/dot_general | solution.py:137
  65.4 0.7 reshape.338
  66.1 8.4 %reduce-scatter.2.cloned.1.call-done = bf16[512,256]{0,1:T(8,128)(2,1)} async-done(((bf16[1024,256]{0,1:T(8,128)(2,1)}), bf16[512,256]{0,1:T(8,128)(2,1)}) %reduce-scatter.2.cloned.1.call-update) | async-done | bytes 262160 | tf_op jit(solution)/shard_map/reduce_scatter | solution.py:139
  (59 shorter events, 1.0 us)
Async XLA Ops:
  7.2 35.7 %copy-start = (bf16[1024,512]{1,0:T(8,128)(2,1)S(1)}, bf16[1024,512]{1,0:T(8,128)(2,1)}, u32[]{:S(2)}) copy-start(bf16[1024,512]{1,0:T(8,128)(2,1)} %param.13) | copy-start | bytes 3145732
  7.2 4.3 %copy-start.3 = (f32[1024]{0:T(1024)S(1)}, f32[1024]{0:T(1024)}, u32[]{:S(2)}) copy-start(f32[1024]{0:T(1024)} %param.12) | copy-start | bytes 12292
  7.2 4.3 %copy-start.6 = (bf16[1024,128]{1,0:T(8,128)(2,1)S(1)}, bf16[1024,128]{1,0:T(8,128)(2,1)}, u32[]{:S(2)}) copy-start(bf16[1024,128]{1,0:T(8,128)(2,1)} %param.14) | copy-start | bytes 786436
  7.2 4.7 %copy-start.4 = (f32[64]{0:T(128)S(1)}, f32[64]{0:T(128)}, u32[]{:S(2)}) copy-start(f32[64]{0:T(128)} %param.17) | copy-start | bytes 772
  7.2 67.2 %reduce-scatter.2.cloned.1.call-start = ((), (), s32[]{:S(2)}) async-start(), calls=%async_computation.1 | async-start | bytes 786432 | tf_op jit(solution)/shard_map/reduce_scatter | solution.py:139
  44.1 2.0 %copy-start.5 = (f32[64]{0:T(128)S(1)}, f32[64]{0:T(128)}, u32[]{:S(2)}) copy-start(f32[64]{0:T(128)} %param.16) | copy-start | bytes 772
  44.3 2.9 %copy-start.2 = (s32[1,8,16]{2,1,0:T(8,128)S(1)}, s32[1,8,16]{2,1,0:T(8,128)}, u32[]{:S(2)}) copy-start(s32[1,8,16]{2,1,0:T(8,128)} %param.19) | copy-start | bytes 1540
  62.9 1.2 %copy-start.1 = (bf16[512,1024]{1,0:T(8,128)(2,1)S(1)}, bf16[512,1024]{1,0:T(8,128)(2,1)}, u32[]{:S(2)}) copy-start(bf16[512,1024]{1,0:T(8,128)(2,1)} %param.18) | copy-start | bytes 3145732
Sparse Core Ops, SparseCore 0:
  65.5 8.8 reduce-scatter.1
where the time goes:
time: 81.6 us; the launch traced here: 81.3 us
  blocking collectives  33.4 us (41%)
  between operations  14.3 us (18%)
  matrix products  13.8 us (17%)
  waiting for transfers between devices  8.37 us (10%)
  other arithmetic  6.92 us (8%)
  local copies, waits for them, and re-layouts  4.09 us (5%)
    all_gather x1, blocking collectives, shards(): lax.all_gather(key_rows, 'kv', axis=1, tiled=True)  16.2 us
    all_gather x1, blocking collectives, shards(): lax.all_gather(value_rows, 'kv', axis=1, tiled=True)  14.6 us
    reduce_scatter x1, waiting for transfers between devices, shards(): lax.psum_scatter(project().astype(jnp.bfloat16), 'tp', scatter_dimension=...  8.35 us
    dot_general x4, matrix products, absorb(): jnp.einsum('sbqkgd,snkd->skgbqn', queries, span_keys, preferred_element_t...  6.99 us
    another operation x4, other arithmetic  3.33 us
    all_gather x1, blocking collectives, shards(): gathered = lax.all_gather(tokens, 'tp', axis=2, tiled=True)  2.64 us
    dot_general x4, matrix products, absorb(): jnp.einsum('skgbqn,snkd->skgbqd', weights.astype(jnp.bfloat16), span_valu...  2.6 us
  transfers between devices with their start and end apart: 1, of which 1 were waited for; matrix products, arithmetic and copies ran while one was open for 1% of the time, Pallas kernels for 0%

commit v1 on v0

--- a/solution.py
+++ b/solution.py
@@ -123,7 +123,7 @@
         initial,
         (
             lax.all_gather(key_rows, "kv", axis=1, tiled=True),
-            lax.all_gather(value_rows, "kv", axis=1, tiled=True),
+            jnp.concatenate(lax.all_gather(value_rows, "kv"), axis=1),
         ),
         jnp.int32(0),
     )

time: 81.6 us -> 81.7 us (level)
  no operation moved by 1% of the time
where the time goes in v1:
time: 81.7 us; the launch traced here: 81.4 us
  blocking collectives  33.4 us (41%)
  between operations  14.3 us (18%)
  matrix products  13.9 us (17%)
  waiting for transfers between devices  8.4 us (10%)
  other arithmetic  6.92 us (8%)
  local copies, waits for them, and re-layouts  4.12 us (5%)
    all_gather x1, blocking collectives, shards(): lax.all_gather(key_rows, 'kv', axis=1, tiled=True)  16.2 us
    all_gather x1, blocking collectives, shards(): lax.all_gather(value_rows, 'kv')  14.6 us
    reduce_scatter x1, waiting for transfers between devices, shards(): lax.psum_scatter(project().astype(jnp.bfloat16), 'tp', scatter_dimension=...  8.38 us
    dot_general x4, matrix products, absorb(): jnp.einsum('sbqkgd,snkd->skgbqn', queries, span_keys, preferred_element_t...  6.99 us
    another operation x4, other arithmetic  3.33 us
    all_gather x1, blocking collectives, shards(): gathered = lax.all_gather(tokens, 'tp', axis=2, tiled=True)  2.64 us
    dot_general x4, matrix products, absorb(): jnp.einsum('skgbqn,snkd->skgbqd', weights.astype(jnp.bfloat16), span_valu...  2.62 us
  transfers between devices with their start and end apart: 1, of which 1 were waited for; matrix products, arithmetic and copies ran while one was open for 1% of the time, Pallas kernels for 0%

profile of v1, /device:TPU:0, one launch (start us, length us, event | category | flops | bytes accessed | tf_op | source)
XLA Modules:
  0.0 81.4 jit_solution(15955463828684804810)
XLA Ops:
  7.3 2.6 %all_gather.9 = bf16[1,256,1024]{2,1,0:T(8,128)(2,1)S(1)} all-gather(bf16[1,256,512]{2,1,0:T(8,128)(2,1)} %param.11), channel_id=1, replica_groups=mesh['dp'=4,'kv'=4,'tp'=2] {'tp'}, dimensions={2}, use_global_device_ids=true | all-gather | bytes 786432 | tf_op jit(solution)/shard_map/all_gather | solution.py:24
  9.9 0.2 fusion.20
  10.1 1.4 %convolution_convert_fusion.1 = bf16[256,128]{0,1:T(8,128)(2,1)S(1)} fusion(bf16[1024,128]{1,0:T(8,128)(2,1)} %param.15, bf16[1,256,1024]{2,1,0:T(8,128)(2,1)S(1)} %all_gather.9, f32[1024]{0:T(1024)} %param.12, f32[256]{0:T(256)S(1)} %add_rsqrt_fusion.2), kind=kOutput, calls=%fused_computation.39 | convolution fusion | flops 68190208 | bytes 857088 | tf_op jit(solution)/shard_map/dot_general | solution.py:53
  11.5 0.4 fusion.30
  12.0 0.1 multiply_convert_fusion
  12.0 16.2 %all_gather.10 = bf16[1,1024,2,64]{1,3,2,0:T(8,128)(2,1)} all-gather(bf16[1,256,2,64]{1,3,2,0:T(8,128)(2,1)S(1)} %multiply_convert_fusion), channel_id=1, replica_groups=mesh['dp'=4,'kv'=4,'tp'=2] {'kv'}, dimensions={1}, use_global_device_ids=true | all-gather | bytes 327680 | tf_op jit(solution)/shard_map/all_gather | solution.py:125
  28.3 14.6 %all_gather.11 = bf16[4,1,256,2,64]{2,4,3,1,0:T(8,128)(2,1)S(1)} all-gather(bf16[1,1,256,2,64]{2,4,3,1,0:T(8,128)(2,1)S(1)} %bitcast.103), channel_id=1, replica_groups=mesh['dp'=4,'kv'=4,'tp'=2] {'kv'}, dimensions={0}, use_global_device_ids=true | all-gather | bytes 327680 | tf_op jit(solution)/shard_map/all_gather | solution.py:126
  42.9 1.3 %fusion.33 = (f32[256,512]{1,0:T(8,128)S(1)}, f32[256,512]{1,0:T(8,128)}) fusion(bf16[1024,512]{1,0:T(8,128)(2,1)S(1)} %copy-done, bf16[1,256,1024]{2,1,0:T(8,128)(2,1)S(1)} %all_gather.9, f32[1024]{0:T(1024)S(1)} %copy-done.3, f32[256]{0:T(256)S(1)} %add_rsqrt_fusion.2), kind=kOutput, calls=%fused_computation.59 | convolution fusion | flops 269615104 | bytes 2626560 | tf_op jit(solution)/shard_map/dot_general | solution.py:41
  44.2 0.2 copy.45
  44.5 1.6 %reshape.336 = f32[1,8,32,2,4,64]{5,4,3,2,1,0:T(4,128)S(1)} reshape(f32[256,512]{1,0:T(8,128)} %get-tuple-element.319) | data formatting | bytes 1048576 | tf_op jit(solution)/shard_map/reshape | solution.py:41
  46.1 1.1 %fusion.24 = bf16[1,8,32,2,4,64]{5,2,4,1,3,0:T(8,128)(2,1)} fusion(f32[1,8,32,2,4,64]{5,4,3,2,1,0:T(4,128)S(1)} %reshape.336, f32[64]{0:T(128)S(1)} %copy-done.5, f32[8,32,2,4]{1,3,0,2:T(4,128)S(1)} %copy.46), kind=kLoop, calls=%fused_computation.45 | loop fusion | flops 393216 | bytes 794880 | tf_op jit(solution)/shard_map/convert_element_type | solution.py:45
  47.3 15.7 %while.20 = (s32[]{:T(128)}, f32[1,2,4,8,32]{4,2,3,1,0:T(4,128)S(1)}, f32[1,2,4,8,32]{4,2,3,1,0:T(4,128)S(1)}, f32[1,2,4,8,32,64]{5,4,3,2,1,0:T(8,128)S(1)}, s32...) while((s32[]{:T(128)}, ...), condition=%wide.region_7.8_spmd.clone, body=%wide.region_3.7_spmd.clone.sunk | while | flops 140261664 | bytes 9419611 | solution.py:120
  47.3 0.1 mul.331
  47.4 0.1 compare_reduce_fusion.2
  47.5 0.1 sub.166
  47.6 0.1 fusion.48
  47.7 0.1 subtract_convert_fusion.2
  47.8 1.7 %fusion.49 = (f32[2,4,8,32]{3,1,2,0:T(4,128)S(1)}, f32[1,2,4,8,32,256]{5,4,2,3,1,0:T(8,128)S(1)}) fusion(f32[8,32,256]{2,1,0:T(8,128)S(1)} %subtract_convert_fusion.2, f32[2,4]{1,0:T(2,128)S(1)} %mul.331, bf16[1,8,32,2,4,64]{5,2,4,1,3,0:T(8,128)(2,1)} %get-tuple-element.431, bf16[1,1024,2,64]{1,3,2,0:T(8,128)(2,1)} %get-tuple-element.430, ...), kind=kOutput, calls=%fused_computation.58.clone.1 | convolution fusion | flops 70252544 | bytes 3022884 | tf_op jit(solution)/shard_map/while/body/eval_jaxpr/sbqkgd,snkd->skgbqn/dot_general | solution.py:72
  49.6 0.8 %fusion.51 = (bf16[2,4,8,32,256]{4,3,1,2,0:T(8,128)(2,1)S(1)}, f32[2,4,8,32]{3,1,2,0:T(4,128)S(1)}) fusion(f32[1,2,4,8,32,256]{5,4,2,3,1,0:T(8,128)S(1)} %get-tuple-element.393, f32[2,4,8,32]{3,1,2,0:T(4,128)S(1)} %bitcast.94, pred[8,32,256]{2,1,0:T(8,128)(4,1)S(1)} %fusion.48), kind=kLoop, calls=%fused_computation.9.clone.1 | loop fusion | flops 2095104 | bytes 3227648 | tf_op jit(solution)/shard_map/reshape.263
  50.5 0.6 fusion.52
  51.2 0.1 mul.331
  51.3 0.1 compare_reduce_fusion.2
  51.5 0.1 fusion.48
  51.6 0.1 subtract_convert_fusion.2
  51.7 1.7 %fusion.49 = (f32[2,4,8,32]{3,1,2,0:T(4,128)S(1)}, f32[1,2,4,8,32,256]{5,4,2,3,1,0:T(8,128)S(1)}) fusion(f32[8,32,256]{2,1,0:T(8,128)S(1)} %subtract_convert_fusion.2, f32[2,4]{1,0:T(2,128)S(1)} %mul.331, bf16[1,8,32,2,4,64]{5,2,4,1,3,0:T(8,128)(2,1)} %get-tuple-element.431, bf16[1,1024,2,64]{1,3,2,0:T(8,128)(2,1)} %get-tuple-element.430, ...), kind=kOutput, calls=%fused_computation.58.clone.1 | convolution fusion | flops 70252544 | bytes 3022884 | tf_op jit(solution)/shard_map/while/body/eval_jaxpr/sbqkgd,snkd->skgbqn/dot_general | solution.py:72
  53.5 0.8 %fusion.51 = (bf16[2,4,8,32,256]{4,3,1,2,0:T(8,128)(2,1)S(1)}, f32[2,4,8,32]{3,1,2,0:T(4,128)S(1)}) fusion(f32[1,2,4,8,32,256]{5,4,2,3,1,0:T(8,128)S(1)} %get-tuple-element.393, f32[2,4,8,32]{3,1,2,0:T(4,128)S(1)} %bitcast.94, pred[8,32,256]{2,1,0:T(8,128)(4,1)S(1)} %fusion.48), kind=kLoop, calls=%fused_computation.9.clone.1 | loop fusion | flops 2095104 | bytes 3227648 | tf_op jit(solution)/shard_map/reshape.263
  54.4 0.7 fusion.52
  55.1 0.1 mul.331
  55.2 0.1 compare_reduce_fusion.2
  55.4 0.1 fusion.48
  55.6 0.1 subtract_convert_fusion.2
  55.7 1.7 %fusion.49 = (f32[2,4,8,32]{3,1,2,0:T(4,128)S(1)}, f32[1,2,4,8,32,256]{5,4,2,3,1,0:T(8,128)S(1)}) fusion(f32[8,32,256]{2,1,0:T(8,128)S(1)} %subtract_convert_fusion.2, f32[2,4]{1,0:T(2,128)S(1)} %mul.331, bf16[1,8,32,2,4,64]{5,2,4,1,3,0:T(8,128)(2,1)} %get-tuple-element.431, bf16[1,1024,2,64]{1,3,2,0:T(8,128)(2,1)} %get-tuple-element.430, ...), kind=kOutput, calls=%fused_computation.58.clone.1 | convolution fusion | flops 70252544 | bytes 3022884 | tf_op jit(solution)/shard_map/while/body/eval_jaxpr/sbqkgd,snkd->skgbqn/dot_general | solution.py:72
  57.5 0.8 %fusion.51 = (bf16[2,4,8,32,256]{4,3,1,2,0:T(8,128)(2,1)S(1)}, f32[2,4,8,32]{3,1,2,0:T(4,128)S(1)}) fusion(f32[1,2,4,8,32,256]{5,4,2,3,1,0:T(8,128)S(1)} %get-tuple-element.393, f32[2,4,8,32]{3,1,2,0:T(4,128)S(1)} %bitcast.94, pred[8,32,256]{2,1,0:T(8,128)(4,1)S(1)} %fusion.48), kind=kLoop, calls=%fused_computation.9.clone.1 | loop fusion | flops 2095104 | bytes 3227648 | tf_op jit(solution)/shard_map/reshape.263
  58.3 0.7 fusion.52
  59.1 0.1 mul.331
  59.2 0.1 compare_reduce_fusion.2
  59.4 0.1 fusion.48
  59.5 0.1 subtract_convert_fusion.2
  59.6 1.7 %fusion.49 = (f32[2,4,8,32]{3,1,2,0:T(4,128)S(1)}, f32[1,2,4,8,32,256]{5,4,2,3,1,0:T(8,128)S(1)}) fusion(f32[8,32,256]{2,1,0:T(8,128)S(1)} %subtract_convert_fusion.2, f32[2,4]{1,0:T(2,128)S(1)} %mul.331, bf16[1,8,32,2,4,64]{5,2,4,1,3,0:T(8,128)(2,1)} %get-tuple-element.431, bf16[1,1024,2,64]{1,3,2,0:T(8,128)(2,1)} %get-tuple-element.430, ...), kind=kOutput, calls=%fused_computation.58.clone.1 | convolution fusion | flops 70252544 | bytes 3022884 | tf_op jit(solution)/shard_map/while/body/eval_jaxpr/sbqkgd,snkd->skgbqn/dot_general | solution.py:72
  61.4 0.8 %fusion.51 = (bf16[2,4,8,32,256]{4,3,1,2,0:T(8,128)(2,1)S(1)}, f32[2,4,8,32]{3,1,2,0:T(4,128)S(1)}) fusion(f32[1,2,4,8,32,256]{5,4,2,3,1,0:T(8,128)S(1)} %get-tuple-element.393, f32[2,4,8,32]{3,1,2,0:T(4,128)S(1)} %bitcast.94, pred[8,32,256]{2,1,0:T(8,128)(4,1)S(1)} %fusion.48), kind=kLoop, calls=%fused_computation.9.clone.1 | loop fusion | flops 2095104 | bytes 3227648 | tf_op jit(solution)/shard_map/reshape.263
  62.3 0.7 fusion.52
  63.0 0.3 fusion.26
  63.3 0.4 copy.50
  63.8 0.3 convert_element_type.92
  64.1 0.1 copy-done.1
  64.2 1.2 %fusion.19 = bf16[1024,256]{0,1:T(8,128)(2,1)} fusion(bf16[256,512]{1,0:T(8,128)(2,1)S(1)} %convert_element_type.92, bf16[512,1024]{1,0:T(8,128)(2,1)S(1)} %copy-done.1), kind=kOutput, calls=%fused_computation.38 | convolution fusion | flops 268697600 | bytes 1835008 | tf_op jit(solution)/shard_map/dot_general | solution.py:137
  65.5 0.7 reshape.338
  66.2 8.4 %reduce-scatter.2.cloned.1.call-done = bf16[512,256]{0,1:T(8,128)(2,1)} async-done(((bf16[1024,256]{0,1:T(8,128)(2,1)}), bf16[512,256]{0,1:T(8,128)(2,1)}) %reduce-scatter.2.cloned.1.call-update) | async-done | bytes 262160 | tf_op jit(solution)/shard_map/reduce_scatter | solution.py:139
  (60 shorter events, 1.0 us)
Async XLA Ops:
  7.2 35.7 %copy-start = (bf16[1024,512]{1,0:T(8,128)(2,1)S(1)}, bf16[1024,512]{1,0:T(8,128)(2,1)}, u32[]{:S(2)}) copy-start(bf16[1024,512]{1,0:T(8,128)(2,1)} %param.13) | copy-start | bytes 3145732
  7.2 4.3 %copy-start.3 = (f32[1024]{0:T(1024)S(1)}, f32[1024]{0:T(1024)}, u32[]{:S(2)}) copy-start(f32[1024]{0:T(1024)} %param.12) | copy-start | bytes 12292
  7.2 4.3 %copy-start.6 = (bf16[1024,128]{1,0:T(8,128)(2,1)S(1)}, bf16[1024,128]{1,0:T(8,128)(2,1)}, u32[]{:S(2)}) copy-start(bf16[1024,128]{1,0:T(8,128)(2,1)} %param.14) | copy-start | bytes 786436
  7.2 4.8 %copy-start.4 = (f32[64]{0:T(128)S(1)}, f32[64]{0:T(128)}, u32[]{:S(2)}) copy-start(f32[64]{0:T(128)} %param.17) | copy-start | bytes 772
  7.2 67.3 %reduce-scatter.2.cloned.1.call-start = ((), (), s32[]{:S(2)}) async-start(), calls=%async_computation.1 | async-start | bytes 786432 | tf_op jit(solution)/shard_map/reduce_scatter | solution.py:139
  44.2 2.0 %copy-start.5 = (f32[64]{0:T(128)S(1)}, f32[64]{0:T(128)}, u32[]{:S(2)}) copy-start(f32[64]{0:T(128)} %param.16) | copy-start | bytes 772
  44.4 2.9 %copy-start.2 = (s32[1,8,16]{2,1,0:T(8,128)S(1)}, s32[1,8,16]{2,1,0:T(8,128)}, u32[]{:S(2)}) copy-start(s32[1,8,16]{2,1,0:T(8,128)} %param.19) | copy-start | bytes 1540
  63.0 1.2 %copy-start.1 = (bf16[512,1024]{1,0:T(8,128)(2,1)S(1)}, bf16[512,1024]{1,0:T(8,128)(2,1)}, u32[]{:S(2)}) copy-start(bf16[512,1024]{1,0:T(8,128)(2,1)} %param.18) | copy-start | bytes 3145732
Sparse Core Ops, SparseCore 0:
  65.6 8.9 reduce-scatter.1
